TPU v7x, 32 devices: a whole 2x2x4 slice. The times are simulated.
32 devices in a mesh: sp: 8 (over z, y), tp: 4 (over x, core).
Axes of the slice: x: 2, y: 2, z: 4, core: 2. Of those that a mesh axis runs over, the one named last changes fastest.
Arguments:
- tokens: bfloat16 [2048, 2048], P(('sp', 'tp')), may hold values from -6 to 6
- pre_gain: float32 [2048], replicated, may hold values from 0.1 to 1.9
- w_query_ret: bfloat16 [2048, 768], P('sp', 'tp'), may hold values from -0.125 to 0.125
- w_key_ret: bfloat16 [2048, 768], P('sp', 'tp'), may hold values from -0.125 to 0.125
- w_value_ret: bfloat16 [2048, 768], P('sp', 'tp'), may hold values from -0.125 to 0.125
- w_query_att: bfloat16 [2048, 768], P('sp', 'tp'), may hold values from -0.5 to 0.5
- w_key_att: bfloat16 [2048, 256], P('sp', 'tp'), may hold values from -0.125 to 0.125
- w_value_att: bfloat16 [2048, 256], P('sp', 'tp'), may hold values from -0.125 to 0.125
- w_out_ret: bfloat16 [768, 2048], P('tp', 'sp'), may hold values from -0.15625 to 0.15625
- w_out_att: bfloat16 [768, 2048], P('tp', 'sp'), may hold values from -0.15625 to 0.15625
- retain_log: float32 [2048, 12], P('sp', 'tp')
- forget_total: float32 [12, 2048], P('tp'), as said below
Outputs:
- mixed: bfloat16 [2048, 2048], P(('sp', 'tp'))
Inputs may be any that keep to these rules, and one draw needn't show every extreme that they name: `forget_total`: never rises along positions.
All inputs are finite; a program needn't handle non-finite values.
Results may differ from a plain program's by a relative error of at most 0.019.
Values may be sent and summed in bfloat16 or wider, within the bound.
A program may use at most 64 MiB of HBM per device.

v0:
```python
import jax
import jax.numpy as jnp
from jax import lax
from jax.sharding import PartitionSpec as P

HEAD = 64
SPAN = 256
KEY_SPAN = 256
EPS = 1e-06
THETA = 10000.0
HIGH = lax.Precision.HIGHEST


def rotate(field, positions):
    half = field.shape[-1] // 2
    inverse = THETA ** (-jnp.arange(half, dtype=jnp.float32) / half)
    angles = positions[:, None] * inverse[None, :]
    cosine = jnp.cos(angles)[:, None, :]
    sine = jnp.sin(angles)[:, None, :]
    first_half = field[..., :half]
    second_half = field[..., half:]
    return jnp.concatenate(
        [first_half * cosine - second_half * sine, first_half * sine + second_half * cosine],
        axis=-1,
    )


def head_norm(values):
    centre = jnp.mean(values, axis=-1, keepdims=True)
    spread = jnp.mean(jnp.square(values - centre), axis=-1, keepdims=True)
    return (values - centre) * lax.rsqrt(spread + EPS)


def advance(state, pair):
    decay, update = pair
    return (jnp.exp(decay)[:, None, None] * state + update, state)


def body(
    tokens,
    pre_gain,
    w_query_ret,
    w_key_ret,
    w_value_ret,
    w_query_att,
    w_key_att,
    w_value_att,
    w_out_ret,
    w_out_att,
    retain_log,
    forget_total,
):
    rows = tokens.astype(jnp.float32)
    normed = (
        rows * lax.rsqrt(jnp.mean(rows * rows, axis=-1, keepdims=True) + EPS) * pre_gain
    ).astype(jnp.bfloat16)
    gathered = lax.all_gather(normed, "tp", axis=0, tiled=True)
    tok_dev = gathered.shape[0]
    offset = lax.axis_index("sp") * tok_dev
    query_places = offset + jnp.arange(tok_dev, dtype=jnp.int32)
    positions = query_places.astype(jnp.float32)

    def blocked(values):
        return values.reshape((tok_dev // SPAN, SPAN) + values.shape[1:])

    pieces = (
        lax.all_gather(w_query_ret, "sp", axis=0, tiled=True),
        lax.all_gather(w_key_ret, "sp", axis=0, tiled=True),
        lax.all_gather(w_value_ret, "sp", axis=0, tiled=True),
        lax.all_gather(w_query_att, "sp", axis=0, tiled=True),
        lax.all_gather(w_key_att, "sp", axis=0, tiled=True),
        lax.all_gather(w_value_att, "sp", axis=0, tiled=True),
    )
    projected = tuple(
        (jnp.dot(gathered, piece, preferred_element_type=jnp.float32) for piece in pieces)
    )
    heads = retain_log.shape[1]
    shape = (tok_dev, heads, HEAD)
    query = blocked(
        (rotate(projected[0].reshape(shape), positions) * HEAD ** (-0.5)).astype(jnp.bfloat16)
    )
    key_rows = blocked(rotate(projected[1].reshape(shape), positions).astype(jnp.bfloat16))
    value_rows = blocked(projected[2].astype(jnp.bfloat16).reshape(shape))
    within = jnp.cumsum(blocked(retain_log), axis=1)
    causal = jnp.arange(SPAN)[:, None] >= jnp.arange(SPAN)[None, :]
    scores = jnp.einsum("bthd,bshd->bhts", query, key_rows, preferred_element_type=jnp.float32)
    turned = jnp.transpose(within, (0, 2, 1))
    gap = jnp.where(causal, turned[:, :, :, None] - turned[:, :, None, :], 0.0)
    weights = jnp.where(causal, scores * jnp.exp(gap), 0.0).astype(jnp.bfloat16)
    local = jnp.einsum("bhts,bshd->bthd", weights, value_rows, preferred_element_type=jnp.float32)
    last = within[:, -1]
    faded = (key_rows.astype(jnp.float32) * jnp.exp(last[:, None, :] - within)[..., None]).astype(
        jnp.bfloat16
    )
    updates = jnp.einsum("bshd,bshe->bhde", faded, value_rows, preferred_element_type=jnp.float32)
    zero_state = jnp.zeros((heads, HEAD, HEAD), jnp.float32)
    final, _ = lax.scan(advance, zero_state, (last, updates))
    decay_total = jnp.sum(last, axis=0)
    own_state = final.reshape(heads, HEAD * HEAD)
    every_total = lax.all_gather(
        decay_total[None].astype(jnp.bfloat16), "sp", axis=0, tiled=True
    ).astype(jnp.float32)
    every_state = lax.all_gather(
        own_state[None].astype(jnp.bfloat16), "sp", axis=0, tiled=True
    ).astype(jnp.float32)
    device_order = jnp.arange(every_total.shape[0], dtype=jnp.int32)[:, None]
    earlier = device_order < lax.axis_index("sp")
    before = jnp.sum(jnp.where(earlier, every_total, 0.0), axis=0)
    through = jnp.cumsum(every_total, axis=0)
    fading = jnp.where(earlier, jnp.exp(jnp.where(earlier, before[None, :] - through, 0.0)), 0.0)
    incoming = jnp.einsum("jh,jhe->he", fading, every_state, precision=HIGH)
    _, befores = lax.scan(advance, incoming.reshape(heads, HEAD, HEAD), (last, updates))
    lifted = (query.astype(jnp.float32) * jnp.exp(within)[..., None]).astype(jnp.bfloat16)
    carried = jnp.einsum(
        "bthd,bhde->bthe", lifted, befores.astype(jnp.bfloat16), preferred_element_type=jnp.float32
    )
    retained = (
        head_norm((local + carried).reshape(shape))
        .astype(jnp.bfloat16)
        .reshape(tok_dev, heads * HEAD)
    )
    raw_key = projected[4]
    gate_heads = forget_total.shape[0]
    kv_local = raw_key.shape[1] // HEAD
    group = gate_heads // kv_local
    query = (
        (projected[3] * HEAD ** (-0.5)).astype(jnp.bfloat16).reshape(tok_dev, kv_local, group, HEAD)
    )
    key_rows = raw_key.astype(jnp.bfloat16)
    value_rows = projected[5].astype(jnp.bfloat16)
    gate_rows = lax.dynamic_slice_in_dim(forget_total, offset, tok_dev, 1).reshape(
        kv_local, group, tok_dev
    )
    last_row = offset + tok_dev - 1
    init = (
        jnp.zeros((kv_local, group, tok_dev, HEAD), jnp.float32),
        jnp.zeros((kv_local, group, tok_dev), jnp.float32),
    )
    key_piece = lax.all_gather(key_rows, "sp", axis=0, tiled=True)
    value_piece = lax.all_gather(value_rows, "sp", axis=0, tiled=True)
    count = key_piece.shape[0] // KEY_SPAN

    def one_block(index, inner):
        first = index * KEY_SPAN

        def compute(state):
            weighted, total = state
            key_block = lax.dynamic_slice_in_dim(key_piece, index * KEY_SPAN, KEY_SPAN, 0).reshape(
                KEY_SPAN, kv_local, HEAD
            )
            value_block = lax.dynamic_slice_in_dim(
                value_piece, index * KEY_SPAN, KEY_SPAN, 0
            ).reshape(KEY_SPAN, kv_local, HEAD)
            gate_keys = lax.dynamic_slice_in_dim(forget_total, first, KEY_SPAN, 1).reshape(
                kv_local, group, KEY_SPAN
            )
            scores = jnp.einsum(
                "tcgd,scd->cgts", query, key_block, preferred_element_type=jnp.float32
            )
            logits = scores + gate_rows[:, :, :, None] - gate_keys[:, :, None, :]
            allowed = (first + jnp.arange(KEY_SPAN, dtype=jnp.int32))[None, :] <= query_places[
                :, None
            ]
            weights = jnp.exp(jnp.where(allowed, logits, -jnp.inf))
            total = total + jnp.sum(weights, axis=-1)
            weighted = weighted + jnp.einsum(
                "cgts,scd->cgtd",
                weights.astype(jnp.bfloat16),
                value_block,
                preferred_element_type=jnp.float32,
            )
            return (weighted, total)

        def skipped(state):
            return state

        return lax.cond(first <= last_row, compute, skipped, inner)

    weighted, total = lax.fori_loop(0, count, one_block, init)
    result = weighted / total[..., None]
    attended = (
        jnp.transpose(result, (2, 0, 1, 3)).reshape(tok_dev, gate_heads * HEAD).astype(jnp.bfloat16)
    )
    out_ret, out_att = (
        lax.all_gather(w_out_ret, "sp", axis=1, tiled=True),
        lax.all_gather(w_out_att, "sp", axis=1, tiled=True),
    )
    return lax.psum_scatter(
        (
            jnp.dot(retained, out_ret, preferred_element_type=jnp.float32)
            + jnp.dot(attended, out_att, preferred_element_type=jnp.float32)
        ).astype(jnp.bfloat16),
        "tp",
        scatter_dimension=0,
        tiled=True,
    )


def solution(mesh):
    return jax.shard_map(
        body,
        mesh=mesh,
        in_specs=(
            P(("sp", "tp"), None),
            P(),
            P("sp", "tp"),
            P("sp", "tp"),
            P("sp", "tp"),
            P("sp", "tp"),
            P("sp", "tp"),
            P("sp", "tp"),
            P("tp", "sp"),
            P("tp", "sp"),
            P("sp", "tp"),
            P("tp", None),
        ),
        out_specs=P(("sp", "tp"), None),
        check_vma=False,
    )
```

profile of v0, /device:TPU:0, one launch (start us, length us, event | category | flops | bytes accessed | tf_op | source)
XLA Modules:
  0.0 463.0 jit_solution(11235559087776837710)
XLA Ops:
  6.6 1.2 fusion.24
  7.8 1.8 fusion.26
  10.4 0.9 reduce-window.6
  11.7 22.4 %all-gather = bf16[8,1,3]{2,1,0:T(2,128)(2,1)S(1)} all-gather(bf16[1,1,3]{2,1,0:T(2,128)(2,1)S(1)} %slice.47), channel_id=2, replica_groups=mesh['sp'=8,'tp'=4] {'sp'}, dimensions={0}, use_global_device_ids=true | all-gather | bytes 54 | tf_op jit(solution)/shard_map/all_gather | solution.py:100
  35.4 32.9 %all_gather.46 = bf16[2048,64]{0,1:T(8,128)(2,1)} all-gather(bf16[256,64]{0,1:T(8,128)(2,1)S(1)} %copy-done.9), channel_id=1, replica_groups=mesh['sp'=8,'tp'=4] {'sp'}, dimensions={0}, use_global_device_ids=true | all-gather | bytes 294912 | tf_op jit(solution)/shard_map/all_gather | solution.py:71
  68.3 33.0 %all_gather.49 = bf16[2048,64]{0,1:T(8,128)(2,1)} all-gather(bf16[256,64]{0,1:T(8,128)(2,1)S(1)} %copy-done.10), channel_id=1, replica_groups=mesh['sp'=8,'tp'=4] {'sp'}, dimensions={0}, use_global_device_ids=true | all-gather | bytes 294912 | tf_op jit(solution)/shard_map/all_gather | solution.py:72
  101.3 34.4 %all_gather.41 = bf16[2048,192]{0,1:T(8,128)(2,1)} all-gather(bf16[256,192]{0,1:T(8,128)(2,1)S(1)} %copy-done.3), channel_id=1, replica_groups=mesh['sp'=8,'tp'=4] {'sp'}, dimensions={0}, use_global_device_ids=true | all-gather | bytes 884736 | tf_op jit(solution)/shard_map/all_gather | solution.py:67
  135.7 31.8 %all_gather.42 = bf16[2048,192]{0,1:T(8,128)(2,1)S(1)} all-gather(bf16[256,192]{0,1:T(8,128)(2,1)S(1)} %copy-done.4), channel_id=1, replica_groups=mesh['sp'=8,'tp'=4] {'sp'}, dimensions={0}, use_global_device_ids=true | all-gather | bytes 884736 | tf_op jit(solution)/shard_map/all_gather | solution.py:68
  169.2 34.6 %all_gather.40 = bf16[2048,192]{0,1:T(8,128)(2,1)} all-gather(bf16[256,192]{0,1:T(8,128)(2,1)S(1)} %copy-done.5), channel_id=1, replica_groups=mesh['sp'=8,'tp'=4] {'sp'}, dimensions={0}, use_global_device_ids=true | all-gather | bytes 884736 | tf_op jit(solution)/shard_map/all_gather | solution.py:69
  203.7 32.4 %all_gather.48 = bf16[2048,192]{0,1:T(8,128)(2,1)S(1)} all-gather(bf16[256,192]{0,1:T(8,128)(2,1)S(1)} %copy-done.6), channel_id=1, replica_groups=mesh['sp'=8,'tp'=4] {'sp'}, dimensions={0}, use_global_device_ids=true | all-gather | bytes 884736 | tf_op jit(solution)/shard_map/all_gather | solution.py:70
  236.1 32.2 %all_gather.45 = bf16[192,2048]{1,0:T(8,128)(2,1)S(1)} all-gather(bf16[192,256]{1,0:T(8,128)(2,1)S(1)} %copy-done.7), channel_id=1, replica_groups=mesh['sp'=8,'tp'=4] {'sp'}, dimensions={1}, use_global_device_ids=true | all-gather | bytes 884736 | tf_op jit(solution)/shard_map/all_gather | solution.py:185
  268.3 33.8 %all_gather.51 = bf16[192,2048]{1,0:T(8,128)(2,1)} all-gather(bf16[192,256]{1,0:T(8,128)(2,1)S(1)} %copy-done.8), channel_id=1, replica_groups=mesh['sp'=8,'tp'=4] {'sp'}, dimensions={1}, use_global_device_ids=true | all-gather | bytes 884736 | tf_op jit(solution)/shard_map/all_gather | solution.py:186
  302.1 1.8 convolution_convert_fusion.2
  303.9 32.8 %all_gather.47 = bf16[2048,64]{0,1:T(8,128)(2,1)} all-gather(bf16[256,64]{0,1:T(8,128)(2,1)S(1)} %convolution_convert_fusion.2), channel_id=1, replica_groups=mesh['sp'=8,'tp'=4] {'sp'}, dimensions={0}, use_global_device_ids=true | all-gather | bytes 294912 | tf_op jit(solution)/shard_map/all_gather | solution.py:139
  336.7 1.7 convolution_convert_fusion.1
  338.4 32.7 %all_gather.50 = bf16[2048,64]{0,1:T(8,128)(2,1)} all-gather(bf16[256,64]{0,1:T(8,128)(2,1)S(1)} %convolution_convert_fusion.1), channel_id=1, replica_groups=mesh['sp'=8,'tp'=4] {'sp'}, dimensions={0}, use_global_device_ids=true | all-gather | bytes 294912 | tf_op jit(solution)/shard_map/all_gather | solution.py:140
  371.2 1.7 fusion.56
  374.4 30.7 %all_gather.44 = bf16[8,3,4096]{2,1,0:T(4,128)(2,1)S(1)} all-gather(bf16[1,3,4096]{2,1,0:T(4,128)(2,1)S(1)} %add_convert_fusion.1), channel_id=1, replica_groups=mesh['sp'=8,'tp'=4] {'sp'}, dimensions={0}, use_global_device_ids=true | all-gather | bytes 221184 | tf_op jit(solution)/shard_map/all_gather | solution.py:103
  407.2 3.4 while.10
  407.2 3.0 conditional.3
  408.0 1.2 fusion.55
  409.2 1.0 fusion.6
  411.7 1.4 fusion.16
  413.2 42.9 %reduce-scatter.2.cloned.1.call-done = bf16[64,2048]{1,0:T(8,128)(2,1)} async-done(((bf16[256,2048]{1,0:T(8,128)(2,1)}), bf16[64,2048]{1,0:T(8,128)(2,1)}) %reduce-scatter.2.cloned.1.call-update) | async-done | bytes 262160 | tf_op jit(solution)/shard_map/reduce_scatter | solution.py:188
  (99 shorter events, 9.5 us)
Async XLA Ops:
  6.5 28.8 %copy-start.9 = (bf16[256,64]{0,1:T(8,128)(2,1)S(1)}, bf16[256,64]{0,1:T(8,128)(2,1)}, u32[]{:S(2)}) copy-start(bf16[256,64]{0,1:T(8,128)(2,1)} %param.22) | copy-start | bytes 98308
  6.5 61.7 %copy-start.10 = (bf16[256,64]{0,1:T(8,128)(2,1)S(1)}, bf16[256,64]{0,1:T(8,128)(2,1)}, u32[]{:S(2)}) copy-start(bf16[256,64]{0,1:T(8,128)(2,1)} %param.23) | copy-start | bytes 98308
  6.5 94.8 %copy-start.3 = (bf16[256,192]{0,1:T(8,128)(2,1)S(1)}, bf16[256,192]{0,1:T(8,128)(2,1)}, u32[]{:S(2)}) copy-start(bf16[256,192]{0,1:T(8,128)(2,1)} %param.18) | copy-start | bytes 294916
  6.5 129.2 %copy-start.4 = (bf16[256,192]{0,1:T(8,128)(2,1)S(1)}, bf16[256,192]{0,1:T(8,128)(2,1)}, u32[]{:S(2)}) copy-start(bf16[256,192]{0,1:T(8,128)(2,1)} %param.19) | copy-start | bytes 294916
  6.5 295.6 %all-gather.3.cloned.1.call-start = ((), (), s32[]{:S(2)}) async-start(), calls=%async_computation.1 | async-start | bytes 1310720 | tf_op jit(solution)/shard_map/all_gather | solution.py:57
  9.6 159.6 %copy-start.5 = (bf16[256,192]{0,1:T(8,128)(2,1)S(1)}, bf16[256,192]{0,1:T(8,128)(2,1)}, u32[]{:S(2)}) copy-start(bf16[256,192]{0,1:T(8,128)(2,1)} %param.20) | copy-start | bytes 294916
  9.6 446.5 %reduce-scatter.2.cloned.1.call-start = ((), (), s32[]{:S(2)}) async-start(), calls=%async_computation.2 | async-start | bytes 1310720 | tf_op jit(solution)/shard_map/reduce_scatter | solution.py:188
  11.7 192.0 %copy-start.6 = (bf16[256,192]{0,1:T(8,128)(2,1)S(1)}, bf16[256,192]{0,1:T(8,128)(2,1)}, u32[]{:S(2)}) copy-start(bf16[256,192]{0,1:T(8,128)(2,1)} %param.21) | copy-start | bytes 294916
  35.4 200.7 %copy-start.7 = (bf16[192,256]{1,0:T(8,128)(2,1)S(1)}, bf16[192,256]{1,0:T(8,128)(2,1)}, u32[]{:S(2)}) copy-start(bf16[192,256]{1,0:T(8,128)(2,1)} %param.24) | copy-start | bytes 294916
  101.3 167.0 %copy-start.8 = (bf16[192,256]{1,0:T(8,128)(2,1)S(1)}, bf16[192,256]{1,0:T(8,128)(2,1)}, u32[]{:S(2)}) copy-start(bf16[192,256]{1,0:T(8,128)(2,1)} %param.25) | copy-start | bytes 294916
  302.1 69.1 %copy-start = (bf16[256,2048]{1,0:T(8,128)(2,1)S(1)}, bf16[256,2048]{1,0:T(8,128)(2,1)}, u32[]{:S(2)}) copy-start(bf16[256,2048]{1,0:T(8,128)(2,1)} %all-gather.3.cloned.1.call-done) | copy-start | bytes 3145732
  371.2 2.3 copy-start.1
  373.4 0.9 copy-start.12
  373.4 32.3 %copy-start.11 = (f32[3,256]{1,0:T(4,128)S(1)}, f32[3,256]{1,0:T(4,128)}, u32[]{:S(2)}) copy-start(f32[3,256]{1,0:T(4,128)} %bitcast_add_fusion.2) | copy-start | bytes 9220
  410.6 1.1 copy-start.2
Sparse Core Ops, SparseCore 0:
  9.7 19.4 all-gather.2
  413.3 42.7 reduce-scatter.1
where the time goes:
time: 465 us; the launch traced here: 463 us
  blocking collectives  384 us (83%)
  waiting for transfers between devices  43 us (9%)
  between operations  13.7 us (3%)
  matrix products  12.1 us (3%)
  other arithmetic  6.14 us (1%)
    reduce_scatter x1, waiting for transfers between devices, body(): lax.psum_scatter((jnp.dot(retained, out_ret, preferred_element_type=jnp.f...  42.9 us
    all_gather x1, blocking collectives, body(): lax.all_gather(w_value_ret, 'sp', axis=0, tiled=True)  34.6 us
    all_gather x1, blocking collectives, body(): lax.all_gather(w_query_ret, 'sp', axis=0, tiled=True)  34.4 us
    all_gather x1, blocking collectives, body(): lax.all_gather(w_out_att, 'sp', axis=1, tiled=True)  33.8 us
    all_gather x1, blocking collectives, body(): lax.all_gather(w_value_att, 'sp', axis=0, tiled=True)  33 us
    all_gather x1, blocking collectives, body(): lax.all_gather(w_key_att, 'sp', axis=0, tiled=True)  32.9 us
    all_gather x1, blocking collectives, body(): key_piece = lax.all_gather(key_rows, 'sp', axis=0, tiled=True)  32.8 us
    all_gather x1, blocking collectives, body(): value_piece = lax.all_gather(value_rows, 'sp', axis=0, tiled=True)  32.7 us
  transfers between devices with their start and end apart: 2, of which 1 were waited for; matrix products, arithmetic and copies ran while one was open for 1% of the time, Pallas kernels for 0%

commit v1 on v0

--- a/solution.py
+++ b/solution.py
@@ -50,6 +50,19 @@
     retain_log,
     forget_total,
 ):
+
+    def remake_the_array(packet, which_dim, net_axis):
+        z_new = jnp.concatenate(
+            jax.lax.all_to_all(
+                jnp.stack([packet for _ in range(jax.lax.axis_size(net_axis))]),
+                concat_axis=0,
+                split_axis=0,
+                axis_name=net_axis,
+            ),
+            axis=which_dim,
+        )
+        return z_new
+
     rows = tokens.astype(jnp.float32)
     normed = (
         rows * lax.rsqrt(jnp.mean(rows * rows, axis=-1, keepdims=True) + EPS) * pre_gain
@@ -137,7 +150,7 @@
         jnp.zeros((kv_local, group, tok_dev), jnp.float32),
     )
     key_piece = lax.all_gather(key_rows, "sp", axis=0, tiled=True)
-    value_piece = lax.all_gather(value_rows, "sp", axis=0, tiled=True)
+    value_piece = remake_the_array(value_rows, 0, "sp")
     count = key_piece.shape[0] // KEY_SPAN
 
     def one_block(index, inner):

time: 465 us -> 437 us (0.940)
  blocking collectives: 384 us -> 350 us
    all_gather x1 -> x0, blocking collectives: 32.7 us -> none  [body(): value_piece = lax.all_gather(value_rows, 'sp', axis=0, tiled=True)]
  transfers between devices with their start and end apart: 2 -> 3, of which waited for: 1 -> 1; matrix products, arithmetic and copies ran while one was open for 1% -> 4% of each run, Pallas kernels for 0% -> 0%
where the time goes in v1:
time: 437 us; the launch traced here: 436 us
  blocking collectives  350 us (80%)
  waiting for transfers between devices  41.5 us (9%)
  matrix products  13.8 us (3%)
  between operations  13.7 us (3%)
  other arithmetic  8.73 us (2%)
    reduce_scatter x1, waiting for transfers between devices, body(): lax.psum_scatter((jnp.dot(retained, out_ret, preferred_element_type=jnp.f...  41.5 us
    all_gather x1, blocking collectives, body(): lax.all_gather(w_value_ret, 'sp', axis=0, tiled=True)  34.7 us
    all_gather x1, blocking collectives, body(): lax.all_gather(w_query_ret, 'sp', axis=0, tiled=True)  34.6 us
    all_gather x1, blocking collectives, body(): lax.all_gather(w_key_ret, 'sp', axis=0, tiled=True)  34 us
    all_gather x1, blocking collectives, body(): lax.all_gather(w_out_att, 'sp', axis=1, tiled=True)  34 us
    all_gather x1, blocking collectives, body(): key_piece = lax.all_gather(key_rows, 'sp', axis=0, tiled=True)  32.7 us
    all_gather x1, blocking collectives, body(): lax.all_gather(w_query_att, 'sp', axis=0, tiled=True)  32.3 us
    all_gather x1, blocking collectives, body(): lax.all_gather(w_out_ret, 'sp', axis=1, tiled=True)  32.2 us
  transfers between devices with their start and end apart: 3, of which 1 were waited for; matrix products, arithmetic and copies ran while one was open for 4% of the time, Pallas kernels for 0%

profile of v1, /device:TPU:0, one launch (start us, length us, event | category | flops | bytes accessed | tf_op | source)
XLA Modules:
  0.0 435.9 jit_solution(9281071471277855378)
XLA Ops:
  6.6 1.2 fusion.24
  7.8 1.8 fusion.26
  12.3 22.4 %all-gather = bf16[8,1,3]{2,1,0:T(2,128)(2,1)S(1)} all-gather(bf16[1,1,3]{2,1,0:T(2,128)(2,1)S(1)} %slice.47), channel_id=2, replica_groups=mesh['sp'=8,'tp'=4] {'sp'}, dimensions={0}, use_global_device_ids=true | all-gather | bytes 54 | tf_op jit(solution)/shard_map/all_gather | solution.py:113
  36.0 30.9 %all_gather.43 = bf16[2048,64]{0,1:T(8,128)(2,1)S(1)} all-gather(bf16[256,64]{0,1:T(8,128)(2,1)S(1)} %copy-done.13), channel_id=1, replica_groups=mesh['sp'=8,'tp'=4] {'sp'}, dimensions={0}, use_global_device_ids=true | all-gather | bytes 294912 | tf_op jit(solution)/shard_map/all_gather | solution.py:84
  66.8 30.9 %all_gather.46 = bf16[2048,64]{0,1:T(8,128)(2,1)S(1)} all-gather(bf16[256,64]{0,1:T(8,128)(2,1)S(1)} %copy-done.14), channel_id=1, replica_groups=mesh['sp'=8,'tp'=4] {'sp'}, dimensions={0}, use_global_device_ids=true | all-gather | bytes 294912 | tf_op jit(solution)/shard_map/all_gather | solution.py:85
  97.7 34.6 %all_gather.38 = bf16[2048,192]{0,1:T(8,128)(2,1)} all-gather(bf16[256,192]{0,1:T(8,128)(2,1)S(1)} %copy-done.4), channel_id=1, replica_groups=mesh['sp'=8,'tp'=4] {'sp'}, dimensions={0}, use_global_device_ids=true | all-gather | bytes 884736 | tf_op jit(solution)/shard_map/all_gather | solution.py:80
  132.3 34.0 %all_gather.39 = bf16[2048,192]{0,1:T(8,128)(2,1)} all-gather(bf16[256,192]{0,1:T(8,128)(2,1)S(1)} %copy-done.5), channel_id=1, replica_groups=mesh['sp'=8,'tp'=4] {'sp'}, dimensions={0}, use_global_device_ids=true | all-gather | bytes 884736 | tf_op jit(solution)/shard_map/all_gather | solution.py:81
  168.7 34.7 %all_gather.37 = bf16[2048,192]{0,1:T(8,128)(2,1)} all-gather(bf16[256,192]{0,1:T(8,128)(2,1)S(1)} %copy-done.6), channel_id=1, replica_groups=mesh['sp'=8,'tp'=4] {'sp'}, dimensions={0}, use_global_device_ids=true | all-gather | bytes 884736 | tf_op jit(solution)/shard_map/all_gather | solution.py:82
  203.3 32.3 %all_gather.45 = bf16[2048,192]{0,1:T(8,128)(2,1)S(1)} all-gather(bf16[256,192]{0,1:T(8,128)(2,1)S(1)} %copy-done.7), channel_id=1, replica_groups=mesh['sp'=8,'tp'=4] {'sp'}, dimensions={0}, use_global_device_ids=true | all-gather | bytes 884736 | tf_op jit(solution)/shard_map/all_gather | solution.py:83
  235.7 32.2 %all_gather.42 = bf16[192,2048]{1,0:T(8,128)(2,1)S(1)} all-gather(bf16[192,256]{1,0:T(8,128)(2,1)S(1)} %copy-done.8), channel_id=1, replica_groups=mesh['sp'=8,'tp'=4] {'sp'}, dimensions={1}, use_global_device_ids=true | all-gather | bytes 884736 | tf_op jit(solution)/shard_map/all_gather | solution.py:198
  267.8 34.0 %all_gather.47 = bf16[192,2048]{1,0:T(8,128)(2,1)} all-gather(bf16[192,256]{1,0:T(8,128)(2,1)S(1)} %copy-done.9), channel_id=1, replica_groups=mesh['sp'=8,'tp'=4] {'sp'}, dimensions={1}, use_global_device_ids=true | all-gather | bytes 884736 | tf_op jit(solution)/shard_map/all_gather | solution.py:199
  301.8 1.8 convolution_convert_fusion.1
  304.3 3.4 all-to-all-start
  307.8 1.7 fusion.56
  309.5 1.6 fusion.57
  313.8 31.2 %all_gather.41 = bf16[8,3,4096]{2,1,0:T(4,128)(2,1)S(1)} all-gather(bf16[1,3,4096]{2,1,0:T(4,128)(2,1)S(1)} %add_convert_fusion.1), channel_id=1, replica_groups=mesh['sp'=8,'tp'=4] {'sp'}, dimensions={0}, use_global_device_ids=true | all-gather | bytes 221184 | tf_op jit(solution)/shard_map/all_gather | solution.py:116
  345.6 2.2 fusion.19
  347.7 1.2 bitcast_reduce_fusion
  350.0 32.7 %all_gather.44 = bf16[2048,64]{0,1:T(8,128)(2,1)} all-gather(bf16[256,64]{0,1:T(8,128)(2,1)S(1)} %convolution_convert_fusion.2), channel_id=1, replica_groups=mesh['sp'=8,'tp'=4] {'sp'}, dimensions={0}, use_global_device_ids=true | all-gather | bytes 294912 | tf_op jit(solution)/shard_map/all_gather | solution.py:152
  383.3 2.7 while.10
  383.3 2.3 conditional.3
  384.2 1.2 fusion.55
  386.1 1.4 fusion.16
  387.5 41.5 %reduce-scatter.2.cloned.1.call-done = bf16[64,2048]{1,0:T(8,128)(2,1)} async-done(((bf16[256,2048]{1,0:T(8,128)(2,1)}), bf16[64,2048]{1,0:T(8,128)(2,1)}) %reduce-scatter.2.cloned.1.call-update) | async-done | bytes 262160 | tf_op jit(solution)/shard_map/reduce_scatter | solution.py:201
  (106 shorter events, 13.0 us)
Async XLA Ops:
  6.5 29.4 %copy-start.13 = (bf16[256,64]{0,1:T(8,128)(2,1)S(1)}, bf16[256,64]{0,1:T(8,128)(2,1)}, u32[]{:S(2)}) copy-start(bf16[256,64]{0,1:T(8,128)(2,1)} %param.22) | copy-start | bytes 98308
  6.5 60.3 %copy-start.14 = (bf16[256,64]{0,1:T(8,128)(2,1)S(1)}, bf16[256,64]{0,1:T(8,128)(2,1)}, u32[]{:S(2)}) copy-start(bf16[256,64]{0,1:T(8,128)(2,1)} %param.23) | copy-start | bytes 98308
  6.5 91.2 %copy-start.4 = (bf16[256,192]{0,1:T(8,128)(2,1)S(1)}, bf16[256,192]{0,1:T(8,128)(2,1)}, u32[]{:S(2)}) copy-start(bf16[256,192]{0,1:T(8,128)(2,1)} %param.18) | copy-start | bytes 294916
  6.5 125.8 %copy-start.5 = (bf16[256,192]{0,1:T(8,128)(2,1)S(1)}, bf16[256,192]{0,1:T(8,128)(2,1)}, u32[]{:S(2)}) copy-start(bf16[256,192]{0,1:T(8,128)(2,1)} %param.19) | copy-start | bytes 294916
  6.5 295.2 %all-gather.3.cloned.1.call-start = ((), (), s32[]{:S(2)}) async-start(), calls=%async_computation.2 | async-start | bytes 1310720 | tf_op jit(solution)/shard_map/all_gather | solution.py:70
  9.6 159.1 %copy-start.6 = (bf16[256,192]{0,1:T(8,128)(2,1)S(1)}, bf16[256,192]{0,1:T(8,128)(2,1)}, u32[]{:S(2)}) copy-start(bf16[256,192]{0,1:T(8,128)(2,1)} %param.20) | copy-start | bytes 294916
  12.3 191.1 %copy-start.7 = (bf16[256,192]{0,1:T(8,128)(2,1)S(1)}, bf16[256,192]{0,1:T(8,128)(2,1)}, u32[]{:S(2)}) copy-start(bf16[256,192]{0,1:T(8,128)(2,1)} %param.21) | copy-start | bytes 294916
  36.0 199.7 %copy-start.8 = (bf16[192,256]{1,0:T(8,128)(2,1)S(1)}, bf16[192,256]{1,0:T(8,128)(2,1)}, u32[]{:S(2)}) copy-start(bf16[192,256]{1,0:T(8,128)(2,1)} %param.24) | copy-start | bytes 294916
  97.7 170.1 %copy-start.9 = (bf16[192,256]{1,0:T(8,128)(2,1)S(1)}, bf16[192,256]{1,0:T(8,128)(2,1)}, u32[]{:S(2)}) copy-start(bf16[192,256]{1,0:T(8,128)(2,1)} %param.25) | copy-start | bytes 294916
  301.8 6.0 %copy-start = (bf16[256,2048]{1,0:T(8,128)(2,1)S(1)}, bf16[256,2048]{1,0:T(8,128)(2,1)}, u32[]{:S(2)}) copy-start(bf16[256,2048]{1,0:T(8,128)(2,1)} %all-gather.3.cloned.1.call-done) | copy-start | bytes 3145732
  304.3 78.9 %all-to-all-start = ((bf16[8,256,64]{1,2,0:T(8,128)(2,1)}), bf16[8,256,64]{1,2,0:T(8,128)(2,1)S(1)}, u32[]{:S(2)}, u32[]{:S(2)}) async-start(bf16[8,256,64]{1,2,0:T(8,128)(2,1)} %stack.2), calls=%async_computation | async-start | bytes 524288 | tf_op jit(solution)/shard_map/all_to_all | solution.py:56
  307.7 3.4 copy-start.3
  307.7 121.3 %reduce-scatter.2.cloned.1.call-start = ((), (), s32[]{:S(2)}) async-start(), calls=%async_computation.3 | async-start | bytes 1310720 | tf_op jit(solution)/shard_map/reduce_scatter | solution.py:201
  307.8 4.1 copy-start.1
  311.8 0.6 copy-start.11
  311.8 0.6 copy-start.12
  312.4 0.6 copy-start.10
  383.3 2.8 copy-start.2
Sparse Core Ops, SparseCore 0:
  9.7 19.4 all-gather.2
  387.6 41.3 reduce-scatter.1
